TPU v7x, 128 devices: a whole 4x4x4 slice. The times are simulated.
128 devices in a mesh: fs: 16 (over z, y), tp: 8 (over x, core).
Axes of the slice: x: 4, y: 4, z: 4, core: 2. Of those that a mesh axis runs over, the one named last changes fastest.
Arguments:
- stream: bfloat16 [16384, 1024], P(('fs', 'tp')), may hold values from -3 to 3
- mixer_out: bfloat16 [16384, 1024], P(('fs', 'tp')), may hold values from -6 to 6
- ffn_gains: float32 [4, 1024], replicated, may hold values from 0.5 to 1.5
- mixer_gain: float32 [1024], replicated, may hold values from 0.25 to 0.6
- gate_first: bfloat16 [1024, 2816], P('fs', 'tp'), may hold values from -0.1875 to 0.1875
- up_first: bfloat16 [1024, 2816], P('fs', 'tp'), may hold values from -0.1875 to 0.1875
- down_first: bfloat16 [2816, 1024], P('tp', 'fs'), may hold values from -0.109375 to 0.109375
- gate_second: bfloat16 [1024, 2816], P('fs', 'tp'), may hold values from -0.1875 to 0.1875
- up_second: bfloat16 [1024, 2816], P('fs', 'tp'), may hold values from -0.1875 to 0.1875
- down_second: bfloat16 [2816, 1024], P('tp', 'fs'), may hold values from -0.109375 to 0.109375
Outputs:
- layer_out: bfloat16 [16384, 1024], P(('fs', 'tp'))
All inputs are finite; a program needn't handle non-finite values.
Results may differ from a plain program's by a relative error of at most 0.02.
Values may be sent and summed in bfloat16 or wider, within the bound.
A program may use at most 64 MiB of HBM per device.

v0:
```python
import jax
import jax.numpy as jnp
from jax import lax
from jax.sharding import PartitionSpec as P

epsilon = 1e-06
half_weight = 0.5


def laid_out(blocks, dim):
    dims = list(blocks.shape[1:])
    dims[dim] *= blocks.shape[0]
    return jnp.moveaxis(blocks, 0, dim).reshape(dims)


def gather_together(arrays, axis, dims):
    line = jnp.concatenate([a.reshape(-1) for a in arrays])
    lines, at, gathered = lax.all_gather(line, axis), 0, []
    for a, dim in zip(arrays, dims):
        blocks = lines[:, at : at + a.size].reshape(-1, *a.shape)
        gathered.append(laid_out(blocks, dim))
        at += a.size
    return tuple(gathered)


def on_whole(shard, axis, dim, work):
    return work(lax.all_gather(shard, axis, axis=dim, tiled=True), jnp.int32(0))


def own_rows(portion, rows, axis):
    count = rows * lax.axis_size(axis)
    sent = portion(jnp.int32(0), count).astype(jnp.bfloat16)
    return lax.psum_scatter(sent, axis, scatter_dimension=0, tiled=True).astype(jnp.float32)


def rms_rows(values, gain_row):
    widened = values.astype(jnp.float32)
    inverse_rms = lax.rsqrt(jnp.mean(widened * widened, axis=-1, keepdims=True) + epsilon)
    return (widened * inverse_rms * gain_row.astype(jnp.float32)).astype(jnp.bfloat16)


def add_branch(rows, normed_branch, factor):
    return (rows.astype(jnp.float32) + factor * normed_branch.astype(jnp.float32)).astype(
        jnp.bfloat16
    )


def collect_weights(gate_local, up_local, down_local):
    gate_full, up_full = gather_together((gate_local, up_local), "fs", (0, 0))
    down_full = lax.all_gather(down_local, "fs", axis=1, tiled=True)
    return (gate_full, up_full, down_full)


def half_step(rows, gain_pre, gain_post, weight_set):
    gate_full, up_full, down_full = weight_set
    normed = rms_rows(rows, gain_pre)

    def activate(tokens_part, first_row):
        gate_sum = jnp.dot(tokens_part, gate_full, preferred_element_type=jnp.float32)
        up_sum = jnp.dot(tokens_part, up_full, preferred_element_type=jnp.float32)
        return (jax.nn.silu(gate_sum) * up_sum).astype(jnp.bfloat16)

    hidden = on_whole(normed, "tp", 0, activate)

    def project(first_row, row_count):
        row_block = lax.dynamic_slice_in_dim(hidden, first_row, row_count, 0)
        return jnp.dot(row_block, down_full, preferred_element_type=jnp.float32)

    branch = own_rows(project, normed.shape[0], "tp").astype(jnp.bfloat16)
    return add_branch(rows, rms_rows(branch, gain_post), half_weight)


def body(
    stream,
    mixer_out,
    ffn_gains,
    mixer_gain,
    gate_first,
    up_first,
    down_first,
    gate_second,
    up_second,
    down_second,
):
    first_set = collect_weights(gate_first, up_first, down_first)
    after_first = half_step(stream, ffn_gains[0], ffn_gains[1], first_set)
    mixed_in = add_branch(after_first, rms_rows(mixer_out, mixer_gain), 1.0)
    second_set = collect_weights(gate_second, up_second, down_second)
    return half_step(mixed_in, ffn_gains[2], ffn_gains[3], second_set)


def solution(mesh):
    placed = (
        P(("fs", "tp"), None),
        P(("fs", "tp"), None),
        P(),
        P(),
        P("fs", "tp"),
        P("fs", "tp"),
        P("tp", "fs"),
        P("fs", "tp"),
        P("fs", "tp"),
        P("tp", "fs"),
    )
    return jax.shard_map(
        body, mesh=mesh, in_specs=placed, out_specs=P(("fs", "tp"), None), check_vma=False
    )
```

profile of v0, /device:TPU:0, one launch (start us, length us, event | category | flops | bytes accessed | tf_op | source)
XLA Modules:
  0.0 245.5 jit_solution(8046702978109701361)
XLA Ops:
  6.5 0.0 copy-start.6
  6.5 0.0 copy-start.7
  6.5 0.0 copy-start.4
  6.5 0.0 all-gather.11.cloned.1.call-start
  6.5 0.9 reshape.53
  7.5 0.9 reshape.54
  8.4 0.6 pad_maximum_fusion
  9.1 0.0 all-gather.11.cloned.1.call-update
  9.1 0.0 all-gather.7.cloned.1.call-start
  9.1 1.1 fusion.13
  10.2 0.9 fusion.25
  11.1 1.8 fusion.15
  12.9 0.0 all-gather.7.cloned.1.call-update
  12.9 0.0 all-gather.13.cloned.1.call-start
  13.0 0.0 copy-done.6
  13.0 0.1 reshape.55
  13.1 0.0 copy-done.7
  13.1 0.1 reshape.56
  13.3 0.6 pad_maximum_fusion.1
  13.9 0.0 all-gather.13.cloned.1.call-update
  13.9 0.0 reduce-scatter.3.cloned.1.call-start
  14.0 0.0 copy-done.4
  14.0 28.5 %all_gather.27 = bf16[352,1024]{0,1:T(8,128)(2,1)} all-gather(bf16[352,64]{0,1:T(8,128)(2,1)S(1)} %copy-done.4), channel_id=1, replica_groups=mesh['fs'=16,'tp'=8] {'fs'}, dimensions={1}, use_global_device_ids=true | all-gather | bytes 765952 | tf_op jit(solution)/shard_map/all_gather | solution.py:50
  42.5 13.6 %all-gather.11.cloned.1.call-done = bf16[720896]{0:T(1024)(128)(2,1)} async-done(((bf16[45056]{0:T(1024)(128)(2,1)}), bf16[720896]{0:T(1024)(128)(2,1)}) %all-gather.11.cloned.1.call-update) | async-done | bytes 1441808 | tf_op jit(solution)/shard_map/all_gather | solution.py:18
  56.1 1.7 reshape.57
  57.8 0.1 fusion.24
  57.9 1.2 reshape_reshape.12
  59.1 1.2 reshape_reshape.13
  60.3 0.0 copy-start.3
  60.3 21.8 %all-gather.7.cloned.1.call-done = bf16[1024,1024]{1,0:T(8,128)(2,1)} async-done(((bf16[128,1024]{1,0:T(8,128)(2,1)}), bf16[1024,1024]{1,0:T(8,128)(2,1)}) %all-gather.7.cloned.1.call-update) | async-done | bytes 2097168 | tf_op jit(solution)/shard_map/all_gather | solution.py:27
  82.1 3.7 %fusion.26 = f32[1024,352]{0,1:T(8,128)} fusion(bf16[1024,1024]{1,0:T(8,128)(2,1)} %all-gather.7.cloned.1.call-done, bf16[1024,352]{1,0:T(8,128)(2,1)S(1)} %reshape_reshape.12), kind=kOutput, calls=%fused_computation.50 | convolution fusion | flops 738197504 | bytes 4259840 | tf_op jit(solution)/shard_map/dot_general | solution.py:59
  85.8 0.0 copy-done.3
  85.8 5.6 %convolution_convert_fusion.1 = bf16[1024,1024]{1,0:T(8,128)(2,1)} fusion(bf16[352,1024]{0,1:T(8,128)(2,1)S(1)} %copy-done.3, bf16[1024,1024]{1,0:T(8,128)(2,1)} %all-gather.7.cloned.1.call-done, bf16[1024,352]{1,0:T(8,128)(2,1)S(1)} %reshape_reshape.13, f32[1024,352]{0,1:T(8,128)} %fusion.26), kind=kOutput, calls=%fused_computation.1 | convolution fusion | flops 1479606272 | bytes 7077888 | tf_op jit(solution)/shard_map/dot_general | solution.py:67
  91.4 0.0 copy-start.1
  91.4 0.0 reduce-scatter.3.cloned.1.call-update
  91.4 0.0 all-gather.9.cloned.1.call-start
  91.5 0.9 copy-done.1
  92.4 0.1 fusion.7
  92.5 0.0 copy-done.5
  92.5 27.8 %all_gather.31 = bf16[352,1024]{0,1:T(8,128)(2,1)} all-gather(bf16[352,64]{0,1:T(8,128)(2,1)S(1)} %copy-done.5), channel_id=1, replica_groups=mesh['fs'=16,'tp'=8] {'fs'}, dimensions={1}, use_global_device_ids=true | all-gather | bytes 765952 | tf_op jit(solution)/shard_map/all_gather | solution.py:50
  120.3 0.0 copy-start
  120.3 0.0 copy-start.8
  120.3 8.6 %all-gather.13.cloned.1.call-done = bf16[720896]{0:T(1024)(128)(2,1)} async-done(((bf16[45056]{0:T(1024)(128)(2,1)}), bf16[720896]{0:T(1024)(128)(2,1)}) %all-gather.13.cloned.1.call-update) | async-done | bytes 1441808 | tf_op jit(solution)/shard_map/all_gather | solution.py:18
  129.0 1.7 reshape.58
  130.7 33.3 %reduce-scatter.3.cloned.1.call-done = bf16[128,1024]{1,0:T(8,128)(2,1)} async-done(((bf16[1024,1024]{1,0:T(8,128)(2,1)}), bf16[128,1024]{1,0:T(8,128)(2,1)}) %reduce-scatter.3.cloned.1.call-update) | async-done | bytes 262160 | tf_op jit(solution)/shard_map/reduce_scatter | solution.py:33
  164.0 1.1 fusion.4
  165.1 0.0 copy-done
  165.1 0.0 copy-done.8
  165.1 1.3 fusion.17
  166.5 0.8 fusion.19
  167.3 0.0 all-gather.9.cloned.1.call-update
  167.4 0.2 reduce-scatter.5.cloned.1.call-start
  167.6 0.1 fusion.23
  167.7 2.1 reshape_reshape.14
  169.8 1.2 reshape_reshape.15
  171.0 0.0 copy-start.2
  171.0 20.5 %all-gather.9.cloned.1.call-done = bf16[1024,1024]{1,0:T(8,128)(2,1)} async-done(((bf16[128,1024]{1,0:T(8,128)(2,1)}), bf16[1024,1024]{1,0:T(8,128)(2,1)}) %all-gather.9.cloned.1.call-update) | async-done | bytes 2097168 | tf_op jit(solution)/shard_map/all_gather | solution.py:27
  191.5 3.9 %fusion.27 = f32[1024,352]{0,1:T(8,128)} fusion(bf16[1024,1024]{1,0:T(8,128)(2,1)} %all-gather.9.cloned.1.call-done, bf16[1024,352]{1,0:T(8,128)(2,1)} %reshape_reshape.14), kind=kOutput, calls=%fused_computation.51 | convolution fusion | flops 738197504 | bytes 4259840 | tf_op jit(solution)/shard_map/dot_general | solution.py:59
  195.4 0.0 copy-done.2
  195.4 5.6 %convolution_convert_fusion = bf16[1024,1024]{1,0:T(8,128)(2,1)} fusion(bf16[352,1024]{0,1:T(8,128)(2,1)S(1)} %copy-done.2, bf16[1024,1024]{1,0:T(8,128)(2,1)} %all-gather.9.cloned.1.call-done, bf16[1024,352]{1,0:T(8,128)(2,1)S(1)} %reshape_reshape.15, f32[1024,352]{0,1:T(8,128)} %fusion.27), kind=kOutput, calls=%fused_computation | convolution fusion | flops 1479606272 | bytes 7077888 | tf_op jit(solution)/shard_map/dot_general | solution.py:67
  201.0 0.0 reduce-scatter.5.cloned.1.call-update
  201.0 34.7 %reduce-scatter.5.cloned.1.call-done = bf16[128,1024]{1,0:T(8,128)(2,1)} async-done(((bf16[1024,1024]{1,0:T(8,128)(2,1)}), bf16[128,1024]{1,0:T(8,128)(2,1)}) %reduce-scatter.5.cloned.1.call-update) | async-done | bytes 262160 | tf_op jit(solution)/shard_map/reduce_scatter | solution.py:33
  235.7 1.1 fusion.10
  236.8 1.8 fusion.20
  (6 shorter events, 0.0 us)
Async XLA Ops:
  6.5 6.5 %copy-start.6 = (bf16[64,352]{1,0:T(8,128)(2,1)S(1)}, bf16[64,352]{1,0:T(8,128)(2,1)}, u32[]{:S(2)}) copy-start(bf16[64,352]{1,0:T(8,128)(2,1)} %param.17) | copy-start | bytes 135172
  6.5 6.6 %copy-start.7 = (bf16[64,352]{1,0:T(8,128)(2,1)S(1)}, bf16[64,352]{1,0:T(8,128)(2,1)}, u32[]{:S(2)}) copy-start(bf16[64,352]{1,0:T(8,128)(2,1)} %param.18) | copy-start | bytes 135172
  6.5 7.5 %copy-start.4 = (bf16[352,64]{0,1:T(8,128)(2,1)S(1)}, bf16[352,64]{0,1:T(8,128)(2,1)}, u32[]{:S(2)}) copy-start(bf16[352,64]{0,1:T(8,128)(2,1)} %param.16) | copy-start | bytes 135172
  6.5 49.5 %all-gather.11.cloned.1.call-start = ((), (), s32[]{:S(2)}) async-start(), calls=%async_computation.6 | async-start | bytes 1531904 | tf_op jit(solution)/shard_map/all_gather | solution.py:18
  9.1 73.0 %all-gather.7.cloned.1.call-start = ((), (), s32[]{:S(2)}) async-start(), calls=%async_computation.2 | async-start | bytes 2359296 | tf_op jit(solution)/shard_map/all_gather | solution.py:27
  12.9 116.0 %all-gather.13.cloned.1.call-start = ((), (), s32[]{:S(2)}) async-start(), calls=%async_computation.7 | async-start | bytes 1531904 | tf_op jit(solution)/shard_map/all_gather | solution.py:18
  13.9 150.1 %reduce-scatter.3.cloned.1.call-start = ((), (), s32[]{:S(2)}) async-start(), calls=%async_computation.3 | async-start | bytes 2359296 | tf_op jit(solution)/shard_map/reduce_scatter | solution.py:33
  60.3 25.5 %copy-start.3 = (bf16[352,1024]{0,1:T(8,128)(2,1)S(1)}, bf16[352,1024]{0,1:T(8,128)(2,1)}, u32[]{:S(2)}) copy-start(bf16[352,1024]{0,1:T(8,128)(2,1)} %all_gather.27) | copy-start | bytes 2162692
  91.4 0.9 copy-start.1
  91.4 1.1 copy-start.5
  91.4 100.1 %all-gather.9.cloned.1.call-start = ((), (), s32[]{:S(2)}) async-start(), calls=%async_computation.4 | async-start | bytes 2359296 | tf_op jit(solution)/shard_map/all_gather | solution.py:27
  120.3 44.8 %copy-start = (bf16[128,1024]{1,0:T(8,128)(2,1)S(1)}, bf16[128,1024]{1,0:T(8,128)(2,1)}, u32[]{:S(2)}) copy-start(bf16[128,1024]{1,0:T(8,128)(2,1)} %param.10) | copy-start | bytes 786436
  120.3 44.8 %copy-start.8 = (f32[1024]{0:T(1024)S(1)}, f32[1024]{0:T(1024)}, u32[]{:S(2)}) copy-start(f32[1024]{0:T(1024)} %param.13) | copy-start | bytes 12292
  167.4 68.3 %reduce-scatter.5.cloned.1.call-start = ((), (), s32[]{:S(2)}) async-start(), calls=%async_computation.5 | async-start | bytes 2359296 | tf_op jit(solution)/shard_map/reduce_scatter | solution.py:33
  171.0 24.4 %copy-start.2 = (bf16[352,1024]{0,1:T(8,128)(2,1)S(1)}, bf16[352,1024]{0,1:T(8,128)(2,1)}, u32[]{:S(2)}) copy-start(bf16[352,1024]{0,1:T(8,128)(2,1)} %all_gather.31) | copy-start | bytes 2162692
Sparse Core Ops, SparseCore 0:
  9.5 46.5 all-gather.10
  57.8 24.3 all-gather.6
  84.3 44.6 all-gather.12
  131.2 32.7 reduce-scatter.2
  167.5 24.0 all-gather.8
  201.1 34.5 reduce-scatter.4
where the time goes:
time: 246 us; the launch traced here: 245 us
  waiting for transfers between devices  133 us (54%)
  blocking collectives  56.3 us (23%)
  matrix products  18.7 us (8%)
  between operations  13.6 us (6%)
  local copies, waits for them, and re-layouts  13.3 us (5%)
  other arithmetic  10.5 us (4%)
    reduce_scatter x2, waiting for transfers between devices, own_rows(): lax.psum_scatter(sent, axis, scatter_dimension=0, tiled=True)  68 us
    all_gather x2, blocking collectives, collect_weights(): down_full = lax.all_gather(down_local, 'fs', axis=1, tiled=True)  56.3 us
    all_gather x2, waiting for transfers between devices, on_whole(): return work(lax.all_gather(shard, axis, axis=dim, tiled=True), jnp.int32(0))  42.4 us
    all_gather x2, waiting for transfers between devices, gather_together(): lines, at, gathered = (lax.all_gather(line, axis), 0, [])  22.2 us
    dot_general x2, matrix products, project(): return jnp.dot(row_block, down_full, preferred_element_type=jnp.float32)  11.2 us
    dot_general x2, matrix products, activate(): jnp.dot(tokens_part, gate_full, preferred_element_type=jnp.float32)  7.55 us
    another operation x4, local copies, waits for them, and re-layouts, laid_out(): return jnp.moveaxis(blocks, 0, dim).reshape(dims)  5.66 us
  transfers between devices with their start and end apart: 6, of which 6 were waited for; matrix products, arithmetic and copies ran while one was open for 10% of the time, Pallas kernels for 0%

commit v1 on v0

v1 whole, which is shorter than its diff:
```python
import functools

import jax
import jax.numpy as jnp
from jax import lax
from jax.experimental import pallas as pl
from jax.experimental.pallas import tpu as pltpu
from jax.sharding import PartitionSpec as P

EPS = 1e-06
F32 = jnp.float32
BF16 = jnp.bfloat16
D = 1024
TOK = 128
ROWS = 64
HID = 352
PAD = 384
CHUNKS = 4
N = TOK // CHUNKS
H = N // 2
NSEM = 512


def rms(v, gain):
    return v * lax.rsqrt(jnp.mean(v * v, axis=-1, keepdims=True) + EPS) * gain


def dot_t(a, b):
    return lax.dot_general(a, b, (((1,), (1,)), ((), ())), preferred_element_type=F32)


def kernel(
    stream,
    mixer,
    gains,
    mgain,
    g1,
    u1,
    d1,
    g2,
    u2,
    d2,
    out,
    wgu,
    wd,
    xa1,
    xa2,
    hid1,
    hid2,
    psend,
    rin,
    fin,
    mixed,
    mixn,
    ssem,
    rsem,
):
    fs = lax.axis_index("fs")
    tp = lax.axis_index("tp")
    z, y = fs // 4, fs % 4
    x, c = tp // 2, tp % 2

    def unit(dy, dz):
        return ((z + dz + 4) % 4) * 4 + (y + dy + 4) % 4

    def dev(f, t):
        return {"fs": f, "tp": t}

    yp, ym = dev(unit(1, 0), tp), dev(unit(-1, 0), tp)
    zp, zm = dev(unit(0, 1), tp), dev(unit(0, -1), tp)
    xp = dev(fs, ((x + 1) % 4) * 2 + c)
    xm = dev(fs, ((x + 3) % 4) * 2 + c)
    sib = dev(fs, x * 2 + 1 - c)

    barrier = pltpu.get_barrier_semaphore()
    for d in (yp, ym, zp, zm, xp, xm, sib):
        pl.semaphore_signal(
            barrier, inc=1, device_id=d, device_id_type=pl.DeviceIdType.MESH
        )

    me = pl.multiple_of(fs * ROWS, ROWS)
    eye = (
        lax.broadcasted_iota(jnp.int32, (ROWS, ROWS), 0)
        == lax.broadcasted_iota(jnp.int32, (ROWS, ROWS), 1)
    ).astype(BF16)
    for b, (g, u, d) in enumerate(((g1, u1, d1), (g2, u2, d2))):
        mine = pl.ds(me, ROWS)
        wgu[b, 0, mine, :] = jnp.zeros((ROWS, 2 * PAD), BF16)
        wgu[b, 0, mine, 0:HID] = g[...]
        wgu[b, 0, mine, PAD : PAD + HID] = u[...]
        wd[b, mine, 0:PAD] = jnp.zeros((ROWS, PAD), BF16)
        wd[b, mine, 0:HID] = dot_t(eye, d[...]).astype(BF16)
    xa1[0:TOK, :] = rms(stream[...].astype(F32), gains[0:1, :]).astype(BF16)
    mixn[...] = rms(mixer[...].astype(F32), mgain[...]).astype(BF16)

    pl.semaphore_wait(barrier, 7)

    count = [0]
    started = []

    def send(src, dst, to):
        i = count[0]
        count[0] += 1
        copy = pltpu.make_async_remote_copy(
            src_ref=src,
            dst_ref=dst,
            send_sem=ssem.at[i],
            recv_sem=rsem.at[i],
            device_id=to,
            device_id_type=pl.DeviceIdType.MESH,
        )
        copy.start()
        started.append(copy)
        return copy

    class Gather:
        def __init__(self, kind, b):
            self.kind, self.b, self.sib = kind, b, []

        def ref(self, dy, dz, q0, q1, slot=0):
            rows = pl.ds(pl.multiple_of(unit(dy, dz) * ROWS + q0 * 16, 16), (q1 - q0) * 16)
            if self.kind == "gu":
                return wgu.at[self.b, slot, rows, :]
            return wd.at[self.b, rows, slot * PAD : (slot + 1) * PAD]

        def go(self, dy, dz, q0, q1, to):
            r = self.ref(dy, dz, q0, q1)
            return send(r, r, to)

        def share(self, *units):
            for dy, dz in units:
                self.sib.append(
                    send(self.ref(dy, dz, 0, 4), self.ref(dy, dz, 0, 4, 1), sib)
                )

        def w0(self):
            self.a = [self.go(0, 0, 0, 4, t) for t in (yp, ym, zp, zm)]
            self.share((0, 0))

        def w1(self):
            go = self.go
            from_ym, from_yp, from_zm, from_zp = self.a
            from_ym.wait_recv()
            self.y2a = go(-1, 0, 0, 2, yp)
            self.zp = [go(-1, 0, 0, 2, zp)]
            self.zm = [go(-1, 0, 0, 2, zm)]
            from_yp.wait_recv()
            self.y2b = go(1, 0, 2, 4, ym)
            self.zp.append(go(1, 0, 0, 2, zp))
            self.zm.append(go(1, 0, 0, 2, zm))
            from_zm.wait_recv()
            self.z2a = go(0, -1, 0, 2, zp)
            self.yp = [go(0, -1, 2, 4, yp)]
            self.ym = [go(0, -1, 2, 4, ym)]
            from_zp.wait_recv()
            self.z2b = go(0, 1, 2, 4, zm)
            self.yp.append(go(0, 1, 2, 4, yp))
            self.ym.append(go(0, 1, 2, 4, ym))
            self.share((-1, 0), (1, 0), (0, -1), (0, 1))

        def w2(self):
            go = self.go
            self.y2a.wait_recv()
            self.zp.append(go(2, 0, 0, 2, zp))
            self.zm.append(go(2, 0, 0, 2, zm))
            self.z2b.wait_recv()
            self.yp.append(go(0, 2, 2, 4, yp))
            self.ym.append(go(0, 2, 2, 4, ym))
            self.rest = []
            for i, d in enumerate((-1, 1)):
                self.zp[i].wait_recv()
                self.rest.append(go(d, -1, 0, 1, zp))
                self.zm[i].wait_recv()
                self.rest.append(go(d, 1, 1, 2, zm))
                self.yp[i].wait_recv()
                self.rest.append(go(-1, d, 2, 3, yp))
                self.ym[i].wait_recv()
                self.rest.append(go(1, d, 3, 4, ym))
            self.y2b.wait_recv()
            self.z2a.wait_recv()
            self.share((2, 0), (0, 2), (-1, -1), (-1, 1), (1, -1), (1, 1))

        def w3(self):
            go = self.go
            self.zp[2].wait_recv()
            self.rest.append(go(2, -1, 0, 1, zp))
            self.zm[2].wait_recv()
            self.rest.append(go(2, 1, 1, 2, zm))
            self.yp[2].wait_recv()
            self.rest.append(go(-1, 2, 2, 3, yp))
            self.ym[2].wait_recv()
            self.rest.append(go(1, 2, 3, 4, ym))

        def w4(self):
            for r in self.rest:
                r.wait_recv()
            self.share((2, -1), (2, 1), (-1, 2), (1, 2), (2, 2))

        def done(self):
            for r in self.sib:
                r.wait_recv()

    gu1, dn1, gu2, dn2 = (
        Gather("gu", 0),
        Gather("d", 0),
        Gather("gu", 1),
        Gather("d", 1),
    )

    gu1.w0()
    top, bot = slice(0, TOK // 2), slice(TOK // 2, TOK)

    def slot(s, half):
        return xa1.at[pl.ds(s * TOK + half * (TOK // 2), TOK // 2), :]

    r0 = send(slot(0, 0), slot(3, 0), xp)
    l1 = send(slot(0, 1), slot(1, 1), xm)
    r1 = send(slot(0, 1), slot(3, 1), xp)
    l0 = send(slot(0, 0), slot(1, 0), xm)
    dn1.w0()
    gu1.w1()
    r0.wait_recv()
    rr = send(slot(3, 0), slot(2, 0), xp)
    l1.wait_recv()
    ll = send(slot(1, 1), slot(2, 1), xm)
    dn1.w1()
    gu1.w2()
    dn1.w2()
    gu1.w3()
    dn1.w3()
    gu2.w0()
    dn2.w0()
    gu1.w4()
    for t in (r1, l0, rr, ll):
        t.wait_recv()
    gu1.done()

    def hidden(b, rows, xv):
        parts = []
        for s in range(2):
            prod = jnp.dot(xv, wgu[b, s, :, :], preferred_element_type=F32)
            gate, up = prod[:, :PAD], prod[:, PAD:]
            parts.append((gate / (1.0 + jnp.exp(-gate)) * up).astype(BF16))
        return parts

    for i in range(2):
        rows = slice(i * 256, (i + 1) * 256)
        parts = hidden(0, rows, xa1[rows, :])
        for s in range(2):
            hid1[rows, s * PAD : (s + 1) * PAD] = parts[s]

    gu2.w1()
    dn1.w4()
    dn1.done()

    def project(b, k, h):
        part = dot_t(h, wd[b, :, :]).astype(BF16)
        for s in range(4):
            psend[b, k, s, :, :] = part[s * N : (s + 1) * N, :]

    rs = {}

    def half(h):
        return pl.ds(h * H, H)

    def scatter(b, k):
        p, q, f = psend.at[b, k], rin.at[b, k], fin.at[b, k]
        rs[b, k] = [
            send(p.at[2, half(0)], q.at[0], xp),
            send(p.at[2, half(1)], q.at[1], xm),
            send(p.at[1, half(1)], f.at[0, half(1)], xp),
            send(p.at[3, half(0)], f.at[1, half(0)], xm),
        ]

    def relay(b, k):
        p, f = psend.at[b, k], fin.at[b, k]
        a = rs[b, k]
        a[0].wait_recv()
        psend[b, k, 1, half(0), :] = (
            psend[b, k, 1, half(0), :].astype(F32) + rin[b, k, 0, :, :].astype(F32)
        ).astype(BF16)
        a.append(send(p.at[1, half(0)], f.at[0, half(0)], xp))
        a[1].wait_recv()
        psend[b, k, 3, half(1), :] = (
            psend[b, k, 3, half(1), :].astype(F32) + rin[b, k, 1, :, :].astype(F32)
        ).astype(BF16)
        a.append(send(p.at[3, half(1)], f.at[1, half(1)], xm))

    def collect(b, k):
        for t in rs[b, k][2:]:
            t.wait_recv()
        return (
            psend[b, k, 0, :, :].astype(F32)
            + fin[b, k, 0, :, :].astype(F32)
            + fin[b, k, 1, :, :].astype(F32)
        )

    ag = {}

    def middle(k):
        rows = slice(k * N, (k + 1) * N)
        branch = collect(0, k)
        after = (stream[rows, :].astype(F32) + 0.5 * rms(branch, gains[1:2, :])).astype(BF16)
        mix = (after.astype(F32) + mixn[rows, :].astype(F32)).astype(BF16)
        mixed[rows, :] = mix
        xa2[k, 0, :, :] = rms(mix.astype(F32), gains[2:3, :]).astype(BF16)
        a = xa2.at[k]
        ag[k] = [
            send(a.at[0, half(0)], a.at[3, half(0)], xp),
            send(a.at[0, half(1)], a.at[1, half(1)], xm),
            send(a.at[0, half(1)], a.at[3, half(1)], xp),
            send(a.at[0, half(0)], a.at[1, half(0)], xm),
        ]

    def forward(k):
        a = xa2.at[k]
        t = ag[k]
        t[0].wait_recv()
        t.append(send(a.at[3, half(0)], a.at[2, half(0)], xp))
        t[1].wait_recv()
        t.append(send(a.at[1, half(1)], a.at[2, half(1)], xm))

    def second(k):
        for t in ag[k][2:]:
            t.wait_recv()
        parts = hidden(1, None, xa2[k].reshape(4 * N, D))
        for s in range(2):
            hid2[:, s * PAD : (s + 1) * PAD] = parts[s]
        project(1, k, hid2[...])
        scatter(1, k)

    def finish(k):
        rows = slice(k * N, (k + 1) * N)
        branch = collect(1, k)
        out[rows, :] = (
            mixed[rows, :].astype(F32) + 0.5 * rms(branch, gains[3:4, :])
        ).astype(BF16)

    for k in range(CHUNKS):
        h = jnp.concatenate(
            [hid1[s * TOK + k * N : s * TOK + (k + 1) * N, :] for s in range(4)], axis=0
        )
        project(0, k, h)
        scatter(0, k)
    dn2.w1()
    gu2.w2()
    for k in range(CHUNKS):
        relay(0, k)
    dn2.w2()
    gu2.w3()
    for k in range(CHUNKS):
        middle(k)
    dn2.w3()
    for k in range(CHUNKS):
        forward(k)
    gu2.w4()
    dn2.w4()
    gu2.done()
    dn2.done()
    for k in range(CHUNKS):
        second(k)
    for k in range(CHUNKS):
        relay(1, k)
    for k in range(CHUNKS):
        finish(k)
    for t in started:
        t.wait_send()


def body(stream, mixer, gains, mgain, g1, u1, d1, g2, u2, d2):
    vmem = pl.BlockSpec(memory_space=pltpu.VMEM)
    return pl.pallas_call(
        kernel,
        out_shape=jax.ShapeDtypeStruct((TOK, D), BF16),
        in_specs=[vmem] * 10,
        out_specs=vmem,
        scratch_shapes=[
            pltpu.VMEM((2, 2, D, 2 * PAD), BF16),
            pltpu.VMEM((2, D, 2 * PAD), BF16),
            pltpu.VMEM((4 * TOK, D), BF16),
            pltpu.VMEM((CHUNKS, 4, N, D), BF16),
            pltpu.VMEM((4 * TOK, 2 * PAD), BF16),
            pltpu.VMEM((4 * N, 2 * PAD), BF16),
            pltpu.VMEM((2, CHUNKS, 4, N, D), BF16),
            pltpu.VMEM((2, CHUNKS, 2, H, D), BF16),
            pltpu.VMEM((2, CHUNKS, 2, N, D), BF16),
            pltpu.VMEM((TOK, D), BF16),
            pltpu.VMEM((TOK, D), BF16),
            pltpu.SemaphoreType.DMA((NSEM,)),
            pltpu.SemaphoreType.DMA((NSEM,)),
        ],
        compiler_params=pltpu.CompilerParams(
            collective_id=0, has_side_effects=True, vmem_limit_bytes=56 * 2**20
        ),
        name="macaron",
    )(stream, mixer, gains, mgain.reshape(1, D), g1, u1, d1, g2, u2, d2)


def solution(mesh):
    placed = (
        P(("fs", "tp"), None),
        P(("fs", "tp"), None),
        P(),
        P(),
        P("fs", "tp"),
        P("fs", "tp"),
        P("tp", "fs"),
        P("fs", "tp"),
        P("fs", "tp"),
        P("tp", "fs"),
    )
    return jax.shard_map(
        body, mesh=mesh, in_specs=placed, out_specs=P(("fs", "tp"), None), check_vma=False
    )
```

time: 246 us -> 77.1 us (0.31)
  waiting for transfers between devices: 133 us -> 0 us
  Pallas kernels: 0 us -> 71.9 us
  blocking collectives: 56.3 us -> 0 us
  matrix products: 18.7 us -> 0 us
  between operations: 13.6 us -> 0.01 us
  other arithmetic: 10.5 us -> 0 us
  local copies, waits for them, and re-layouts: 13.3 us -> 3.97 us
    pallas_call x0 -> x1, Pallas kernels: none -> 71.9 us  [body(): pl.pallas_call(kernel, out_shape=jax.ShapeDtypeStruct((TOK, D), BF16), in...]
    reduce_scatter x2 -> x0, waiting for transfers between devices: 68 us -> none  [own_rows(): lax.psum_scatter(sent, axis, scatter_dimension=0, tiled=True)]
    all_gather x4 -> x0, waiting for transfers between devices: 64.6 us -> none  [the longest x2 42.4 us: on_whole(): return work(lax.all_gather(shard, axis, axis=dim, tiled=True), jnp.int32(0))]
    all_gather x2 -> x0, blocking collectives: 56.3 us -> none  [collect_weights(): down_full = lax.all_gather(down_local, 'fs', axis=1, tiled=True)]
    dot_general x4 -> x0, matrix products: 18.7 us -> none  [the longest x2 11.2 us: project(): return jnp.dot(row_block, down_full, preferred_element_type=jnp.float32)]
    another operation x4 -> x0, local copies, waits for them, and re-layouts: 5.66 us -> none  [laid_out(): return jnp.moveaxis(blocks, 0, dim).reshape(dims)]
    reduce_sum x5 -> x0, other arithmetic: 4.72 us -> none  [rms_rows(): jnp.mean(widened * widened, axis=-1, keepdims=True) + epsilon]
    convert_element_type x3 -> x0, other arithmetic: 4.47 us -> none  [the longest x2 2.63 us: rms_rows(): (widened * inverse_rms * gain_row.astype(jnp.float32)).astype(jnp.bfloat16)]
  transfers between devices with their start and end apart: 6 -> 0, of which waited for: 6 -> 0; matrix products, arithmetic and copies ran while one was open for 10% -> 0% of each run, Pallas kernels for 0% -> 0%
where the time goes in v1:
time: 77.1 us; the launch traced here: 75.8 us
  Pallas kernels  71.9 us (93%)
  local copies, waits for them, and re-layouts  3.97 us (5%)
    pallas_call x1, Pallas kernels, body(): pl.pallas_call(kernel, out_shape=jax.ShapeDtypeStruct((TOK, D), BF16), in...  71.9 us
    unnamed x5, local copies, waits for them, and re-layouts  3.97 us

profile of v1, /device:TPU:0, one launch (start us, length us, event | category | flops | bytes accessed | tf_op | source)
XLA Modules:
  0.0 75.8 jit_solution(1810839313757535967)
XLA Ops:
  0.0 0.0 copy-start
  0.0 1.5 %copy.11.d1 = bf16[352,64]{1,0:T(8,128)(2,1)} copy(bf16[352,64]{0,1:T(8,128)(2,1)} %param.16) | data formatting | bytes 90112 | tf_op args[6]
  1.5 0.0 copy-done
  1.6 0.7 copy.12.d2
  2.3 71.9 %macaron.1 = bf16[128,1024]{1,0:T(8,128)(2,1)} custom-call(bf16[128,1024]{1,0:T(8,128)(2,1)} %stream.1, bf16[128,1024]{1,0:T(8,128)(2,1)} %mixer.1, f32[4,1024]{1,0:T(4,128)} %gains.1, f32[1,1024]{1,0:T(1,128)} %bitcast.1, bf16[64,352]{1,0:T(8,128)(2,1)} %g1.1, bf16[64,352]{1,0:T(8,128)(2,1)} %u1_.1, bf16[352,64]{1,0:T(8,128)(2,1)} %copy.11.d1, ...), custom_call_target="tpu_custom_call" | custom-call | tf_op jit(solution)/shard_map/macaron/pallas_call | solution.py:372
  74.2 1.7 %copy.14 = bf16[128,1024]{1,0:T(8,128)(2,1)} copy(bf16[128,1024]{1,0:T(8,128)(2,1)} %macaron.1) | data formatting | bytes 524288
Async XLA Ops:
  0.0 1.6 %copy-start = (bf16[352,64]{0,1:T(8,128)(2,1)S(1)}, bf16[352,64]{0,1:T(8,128)(2,1)}, u32[]{:S(2)}) copy-start(bf16[352,64]{0,1:T(8,128)(2,1)} %param.19) | copy-start | bytes 135172

commit v2 on v1

v2 whole, which is shorter than its diff:
```python
import functools

import jax
import jax.numpy as jnp
from jax import lax
from jax.experimental import pallas as pl
from jax.experimental.pallas import tpu as pltpu
from jax.sharding import PartitionSpec as P

EPS = 1e-06
F32 = jnp.float32
BF16 = jnp.bfloat16
D = 1024
TOK = 128
ROWS = 64
HID = 352
PAD = 384
CHUNKS = 4
N = TOK // CHUNKS
H = N // 2
NRECV = 124
NSEND = 12


def rms(v, gain):
    return v * lax.rsqrt(jnp.mean(v * v, axis=-1, keepdims=True) + EPS) * gain


def dot_t(a, b):
    return lax.dot_general(a, b, (((1,), (1,)), ((), ())), preferred_element_type=F32)


def kernel(
    stream_in,
    mixer_in,
    gains_in,
    mgain_in,
    g1,
    u1,
    d1,
    g2,
    u2,
    d2,
    out,
    wgu,
    wd,
    xa1,
    xa2,
    hid1,
    hid2,
    psend,
    rin,
    fin,
    mixed,
    mixn,
    result,
    stream,
    mixer,
    gains,
    mgain,
    shards,
    ssem,
    rsem,
    lsem,
):
    fs = lax.axis_index("fs")
    tp = lax.axis_index("tp")
    z, y = fs // 4, fs % 4
    x, c = tp // 2, tp % 2

    def unit(dy, dz):
        return ((z + dz + 4) % 4) * 4 + (y + dy + 4) % 4

    def dev(f, t):
        return {"fs": f, "tp": t}

    yp, ym = dev(unit(1, 0), tp), dev(unit(-1, 0), tp)
    zp, zm = dev(unit(0, 1), tp), dev(unit(0, -1), tp)
    xp = dev(fs, ((x + 1) % 4) * 2 + c)
    xm = dev(fs, ((x + 3) % 4) * 2 + c)
    sib = dev(fs, x * 2 + 1 - c)

    open_scope = [None]

    def scope(name):
        if open_scope[0] is not None:
            open_scope[0].__exit__(None, None, None)
        open_scope[0] = jax.named_scope(name)
        open_scope[0].__enter__()

    barrier = pltpu.get_barrier_semaphore()
    for d in (yp, ym, zp, zm, xp, xm, sib):
        pl.semaphore_signal(
            barrier, inc=1, device_id=d, device_id_type=pl.DeviceIdType.MESH
        )

    scope("inputs")
    pairs = list(zip((g1, u1, d1, g2, u2, d2), shards))
    pairs += [(stream_in, stream), (gains_in, gains), (mgain_in, mgain), (mixer_in, mixer)]
    loads = [
        pltpu.make_async_copy(src, dst, lsem.at[i]) for i, (src, dst) in enumerate(pairs)
    ]
    for t in loads:
        t.start()
    for t in loads:
        t.wait()
    me = pl.multiple_of(fs * ROWS, ROWS)
    scope("prep")
    for b in range(2):
        g, u, d = shards[3 * b : 3 * b + 3]
        mine = pl.ds(me, ROWS)
        wgu[b, 0, mine, :] = jnp.zeros((ROWS, 2 * PAD), BF16)
        wgu[b, 0, mine, 0:HID] = g[...]
        wgu[b, 0, mine, PAD : PAD + HID] = u[...]
        wd[b, mine, 0:PAD] = jnp.zeros((ROWS, PAD), BF16)
        wd[b, mine, 0:HID] = d[...]
    xa1[0:TOK, :] = rms(stream[...].astype(F32), gains[0:1, :]).astype(BF16)

    scope("barrier")
    pl.semaphore_wait(barrier, 7)

    def remote(src, dst, to, ss, rs):
        return pltpu.make_async_remote_copy(
            src_ref=src,
            dst_ref=dst,
            send_sem=ssem.at[ss],
            recv_sem=rsem.at[rs],
            device_id=to,
            device_id_type=pl.DeviceIdType.MESH,
        )

    class Arrival:
        def __init__(self, whole=None):
            self.i, self.whole = count[0], whole
            count[0] += 1

        def wait(self):
            remote(self.whole, self.whole, sib, 0, self.i).wait_recv()

    class Sends:
        def __init__(self, whole):
            self.i, self.whole = len(groups), whole
            groups.append(self)

        def wait(self):
            remote(self.whole, self.whole, sib, self.i, 0).wait_send()

        def send(self, src, dst, to, arrival=None):
            arrival = arrival or Arrival(dst)
            remote(src, dst, to, self.i, arrival.i).start()
            return arrival

    count, groups = [0], []

    class Gather:
        def __init__(self, kind, b):
            self.kind, self.b = kind, b
            self.links = Sends(self.rows(0, 960))
            self.core = Sends(self.rows(0, D))
            self.far = Arrival(self.rows(0, 64))
            self.rest = Arrival(self.rows(0, 192))
            self.twin = Arrival(self.rows(0, D))

        def rows(self, at, size, slot=0):
            if self.kind == "gu":
                return wgu.at[self.b, slot, pl.ds(at, size), :]
            return wd.at[self.b, pl.ds(at, size), slot * PAD : (slot + 1) * PAD]

        def ref(self, dy, dz, q0, q1, slot=0):
            at = pl.multiple_of(unit(dy, dz) * ROWS + q0 * 16, 16)
            return self.rows(at, (q1 - q0) * 16, slot)

        def go(self, dy, dz, q0, q1, to, arrival=None):
            r = self.ref(dy, dz, q0, q1)
            return self.links.send(r, r, to, arrival)

        def share(self, *units):
            for dy, dz in units:
                self.core.send(
                    self.ref(dy, dz, 0, 4), self.ref(dy, dz, 0, 4, 1), sib, self.twin
                )

        def w0(self):
            self.a = [self.go(0, 0, 0, 4, t) for t in (yp, ym, zp, zm)]
            self.share((0, 0))

        def w1(self):
            go = self.go
            from_ym, from_yp, from_zm, from_zp = self.a
            from_ym.wait()
            self.y2a = go(-1, 0, 0, 2, yp)
            self.zp = [go(-1, 0, 0, 2, zp)]
            self.zm = [go(-1, 0, 0, 2, zm)]
            from_zp.wait()
            self.z2b = go(0, 1, 2, 4, zm)
            self.yp = [go(0, 1, 2, 4, yp)]
            self.ym = [go(0, 1, 2, 4, ym)]
            from_yp.wait()
            go(1, 0, 2, 4, ym, self.far)
            self.zp.append(go(1, 0, 0, 2, zp))
            self.zm.append(go(1, 0, 0, 2, zm))
            from_zm.wait()
            go(0, -1, 0, 2, zp, self.far)
            self.yp.append(go(0, -1, 2, 4, yp))
            self.ym.append(go(0, -1, 2, 4, ym))
            self.share((-1, 0), (1, 0), (0, -1), (0, 1))

        def w2(self):
            go = self.go
            self.y2a.wait()
            self.zp.append(go(2, 0, 0, 2, zp))
            self.zm.append(go(2, 0, 0, 2, zm))
            self.z2b.wait()
            self.yp.append(go(0, 2, 2, 4, yp))
            self.ym.append(go(0, 2, 2, 4, ym))
            for i, d in enumerate((-1, 1)):
                self.zp[i].wait()
                go(d, -1, 0, 1, zp, self.rest)
                self.zm[i].wait()
                go(d, 1, 1, 2, zm, self.rest)
                self.yp[i].wait()
                go(-1, -d, 2, 3, yp, self.rest)
                self.ym[i].wait()
                go(1, -d, 3, 4, ym, self.rest)
            self.share((-1, -1), (-1, 1), (1, -1), (1, 1))

        def w3(self):
            go = self.go
            self.zp[2].wait()
            go(2, -1, 0, 1, zp, self.rest)
            self.zm[2].wait()
            go(2, 1, 1, 2, zm, self.rest)
            self.yp[2].wait()
            go(-1, 2, 2, 3, yp, self.rest)
            self.ym[2].wait()
            go(1, 2, 3, 4, ym, self.rest)
            self.far.wait()
            self.share((2, 0), (0, 2))

        def w4(self):
            self.rest.wait()
            self.share((2, -1), (2, 1), (-1, 2), (1, 2), (2, 2))

        def done(self):
            self.twin.wait()

    gu1, dn1, gu2, dn2 = (
        Gather("gu", 0),
        Gather("d", 0),
        Gather("gu", 1),
        Gather("d", 1),
    )

    tok1 = Sends(xa1.at[pl.ds(0, 384), :])
    end1 = Arrival(xa1.at[pl.ds(0, 256), :])

    def slot(s, part):
        return xa1.at[pl.ds(s * TOK + part * (TOK // 2), TOK // 2), :]

    scope("w0")
    gu1.w0()
    r0 = tok1.send(slot(0, 0), slot(3, 0), xp)
    l1 = tok1.send(slot(0, 1), slot(1, 1), xm)
    tok1.send(slot(0, 1), slot(3, 1), xp, end1)
    tok1.send(slot(0, 0), slot(1, 0), xm, end1)
    dn1.w0()
    scope("gu1_w1")
    gu1.w1()
    scope("ag1_relay")
    r0.wait()
    tok1.send(slot(3, 0), slot(2, 0), xp, end1)
    l1.wait()
    tok1.send(slot(1, 1), slot(2, 1), xm, end1)
    scope("gu1_w2")
    gu1.w2()
    scope("dn1_w1")
    dn1.w1()
    scope("gu1_w3")
    gu1.w3()
    scope("dn1_w2")
    dn1.w2()
    scope("gu1_w4")
    gu1.w4()
    scope("dn1_w3")
    dn1.w3()
    gu2.w0()
    dn2.w0()
    scope("mix")
    mixn[...] = rms(mixer[...].astype(F32), mgain[...]).astype(BF16)
    scope("ag1_end")
    end1.wait()
    scope("gu1_done")
    gu1.done()

    def hidden(b, rows, xv):
        parts = []
        for s in range(2):
            prod = jnp.dot(xv, wgu[b, s, :, :], preferred_element_type=F32)
            gate, up = prod[:, :PAD], prod[:, PAD:]
            parts.append((gate / (1.0 + jnp.exp(-gate)) * up).astype(BF16))
        return parts

    for i in range(2):
        scope(f"hidden1_{i}")
        rows = slice(i * 256, (i + 1) * 256)
        parts = hidden(0, rows, xa1[rows, :])
        for s in range(2):
            hid1[rows, s * PAD : (s + 1) * PAD] = parts[s]
    scope("dn1_w4")
    dn1.w4()
    scope("dn1_done")
    dn1.done()

    def project(b, k, h):
        part = dot_t(h, wd[b, :, :]).astype(BF16)
        for s in range(4):
            psend[b, k, s, :, :] = part[s * N : (s + 1) * N, :]

    rs, ag = {}, {}
    tok2 = Sends(xa2.at[pl.ds(0, CHUNKS * 3 // 4)])
    part = [Sends(psend.at[b, pl.ds(0, CHUNKS * 3 // 4)]) for b in range(2)]

    def half(h):
        return pl.ds(h * H, H)

    def scatter(b, k):
        p, q, f = psend.at[b, k], rin.at[b, k], fin.at[b, k]
        end = Arrival(f)
        rs[b, k] = (
            part[b].send(p.at[2, half(0)], q.at[0], xp),
            part[b].send(p.at[2, half(1)], q.at[1], xm),
            end,
        )
        part[b].send(p.at[1, half(1)], f.at[0, half(1)], xp, end)
        part[b].send(p.at[3, half(0)], f.at[1, half(0)], xm, end)

    def relay(b, k):
        p, f = psend.at[b, k], fin.at[b, k]
        first, last, end = rs[b, k]
        for i, (t, s, to) in enumerate(((first, 1, xp), (last, 3, xm))):
            t.wait()
            psend[b, k, s, half(i), :] = (
                psend[b, k, s, half(i), :].astype(F32) + rin[b, k, i, :, :].astype(F32)
            ).astype(BF16)
            part[b].send(p.at[s, half(i)], f.at[i, half(i)], to, end)

    def collect(b, k):
        rs[b, k][2].wait()
        return (
            psend[b, k, 0, :, :].astype(F32)
            + fin[b, k, 0, :, :].astype(F32)
            + fin[b, k, 1, :, :].astype(F32)
        )

    def middle(k):
        rows = slice(k * N, (k + 1) * N)
        branch = collect(0, k)
        after = (stream[rows, :].astype(F32) + 0.5 * rms(branch, gains[1:2, :])).astype(BF16)
        mix = (after.astype(F32) + mixn[rows, :].astype(F32)).astype(BF16)
        mixed[rows, :] = mix
        xa2[k, 0, :, :] = rms(mix.astype(F32), gains[2:3, :]).astype(BF16)
        a = xa2.at[k]
        end = Arrival(a.at[pl.ds(0, 2)])
        ag[k] = (
            tok2.send(a.at[0, half(0)], a.at[3, half(0)], xp),
            tok2.send(a.at[0, half(1)], a.at[1, half(1)], xm),
            end,
        )
        tok2.send(a.at[0, half(1)], a.at[3, half(1)], xp, end)
        tok2.send(a.at[0, half(0)], a.at[1, half(0)], xm, end)

    def forward(k):
        a = xa2.at[k]
        first, last, end = ag[k]
        first.wait()
        tok2.send(a.at[3, half(0)], a.at[2, half(0)], xp, end)
        last.wait()
        tok2.send(a.at[1, half(1)], a.at[2, half(1)], xm, end)

    def second(k):
        ag[k][2].wait()
        parts = hidden(1, None, xa2[k].reshape(4 * N, D))
        for s in range(2):
            hid2[:, s * PAD : (s + 1) * PAD] = parts[s]
        project(1, k, hid2[...])
        scatter(1, k)

    def finish(k):
        rows = slice(k * N, (k + 1) * N)
        branch = collect(1, k)
        result[rows, :] = (
            mixed[rows, :].astype(F32) + 0.5 * rms(branch, gains[3:4, :])
        ).astype(BF16)
        copy = pltpu.make_async_copy(result.at[rows, :], out.at[rows, :], lsem.at[k])
        copy.start()
        return copy

    def first(k):
        h = jnp.concatenate(
            [hid1[s * TOK + k * N : s * TOK + (k + 1) * N, :] for s in range(4)], axis=0
        )
        project(0, k, h)
        scatter(0, k)

    def step(name, work, *at):
        scope("_".join([name] + [str(i) for i in at]))
        return work(*at)

    step("first", first, 0)
    step("first", first, 1)
    step("gu2_w1", gu2.w1)
    step("first", first, 2)
    step("first", first, 3)
    step("dn2_w1", dn2.w1)
    step("relay1", relay, 0, 0)
    step("relay1", relay, 0, 1)
    step("gu2_w2", gu2.w2)
    step("relay1", relay, 0, 2)
    step("dn2_w2", dn2.w2)
    step("relay1", relay, 0, 3)
    step("middle", middle, 0)
    step("gu2_w3", gu2.w3)
    step("middle", middle, 1)
    step("dn2_w3", dn2.w3)
    step("middle", middle, 2)
    step("middle", middle, 3)
    step("gu2_w4", gu2.w4)
    step("forward", forward, 0)
    step("dn2_w4", dn2.w4)
    for k in range(1, CHUNKS):
        step("forward", forward, k)
    step("gu2_done", gu2.done)
    step("dn2_done", dn2.done)
    for k in range(CHUNKS):
        step("second", second, k)
    for k in range(CHUNKS):
        step("relay2", relay, 1, k)
    copies = [step("finish", finish, k) for k in range(CHUNKS)]
    scope("sends")
    for t in groups:
        t.wait()
    for t in copies:
        t.wait()
    open_scope[0].__exit__(None, None, None)
    assert count[0] <= NRECV and len(groups) <= NSEND, (count, len(groups))


def body(stream, mixer, gains, mgain, g1, u1, d1, g2, u2, d2):
    hbm = pl.BlockSpec(memory_space=pltpu.HBM)
    return pl.pallas_call(
        kernel,
        out_shape=jax.ShapeDtypeStruct((TOK, D), BF16),
        in_specs=[hbm] * 10,
        out_specs=hbm,
        scratch_shapes=[
            pltpu.VMEM((2, 2, D, 2 * PAD), BF16),
            pltpu.VMEM((2, D, 2 * PAD), BF16),
            pltpu.VMEM((4 * TOK, D), BF16),
            pltpu.VMEM((CHUNKS, 4, N, D), BF16),
            pltpu.VMEM((4 * TOK, 2 * PAD), BF16),
            pltpu.VMEM((4 * N, 2 * PAD), BF16),
            pltpu.VMEM((2, CHUNKS, 4, N, D), BF16),
            pltpu.VMEM((2, CHUNKS, 2, H, D), BF16),
            pltpu.VMEM((2, CHUNKS, 2, N, D), BF16),
            pltpu.VMEM((TOK, D), BF16),
            pltpu.VMEM((TOK, D), BF16),
            pltpu.VMEM((TOK, D), BF16),
            pltpu.VMEM((TOK, D), BF16),
            pltpu.VMEM((TOK, D), BF16),
            pltpu.VMEM((4, D), F32),
            pltpu.VMEM((1, D), F32),
            [pltpu.VMEM((ROWS, HID), BF16)] * 6,
            pltpu.SemaphoreType.DMA((NSEND,)),
            pltpu.SemaphoreType.DMA((NRECV,)),
            pltpu.SemaphoreType.DMA((10,)),
        ],
        compiler_params=pltpu.CompilerParams(
            collective_id=0, has_side_effects=True, vmem_limit_bytes=57000000
        ),
        name="macaron",
    )(stream, mixer, gains, mgain.reshape(1, D), g1, u1, d1.T, g2, u2, d2.T)


def solution(mesh):
    placed = (
        P(("fs", "tp"), None),
        P(("fs", "tp"), None),
        P(),
        P(),
        P("fs", "tp"),
        P("fs", "tp"),
        P("tp", "fs"),
        P("fs", "tp"),
        P("fs", "tp"),
        P("tp", "fs"),
    )
    return jax.shard_map(
        body, mesh=mesh, in_specs=placed, out_specs=P(("fs", "tp"), None), check_vma=False
    )
```

time: 77.1 us -> 63 us (0.82)
  Pallas kernels: 71.9 us -> 60.1 us
  local copies, waits for them, and re-layouts: 3.97 us -> 1.67 us
    pallas_call x1, Pallas kernels: 71.9 us -> 60.1 us  [body(): pl.pallas_call(kernel, out_shape=jax.ShapeDtypeStruct((TOK, D), BF16), in...]
    unnamed x5 -> x1, local copies, waits for them, and re-layouts: 3.97 us -> 1.67 us
where the time goes in v2:
time: 63 us; the launch traced here: 61.7 us
  Pallas kernels  60.1 us (95%)
  local copies, waits for them, and re-layouts  1.67 us (3%)
    pallas_call x1, Pallas kernels, body(): pl.pallas_call(kernel, out_shape=jax.ShapeDtypeStruct((TOK, D), BF16), in...  60.1 us
    unnamed x1, local copies, waits for them, and re-layouts  1.67 us

profile of v2, /device:TPU:0, one launch (start us, length us, event | category | flops | bytes accessed | tf_op | source)
XLA Modules:
  0.0 61.7 jit_solution(14990114384694355573)
XLA Ops:
  0.0 60.1 %macaron.1 = bf16[128,1024]{1,0:T(8,128)(2,1)} custom-call(bf16[128,1024]{1,0:T(8,128)(2,1)} %stream_in.1, bf16[128,1024]{1,0:T(8,128)(2,1)} %mixer_in.1, f32[4,1024]{1,0:T(4,128)} %gains_in.1, f32[1,1024]{1,0:T(1,128)} %bitcast.5, bf16[64,352]{1,0:T(8,128)(2,1)} %g1.1, bf16[64,352]{1,0:T(8,128)(2,1)} %u1_.1, bf16[64,352]{1,0:T(8,128)(2,1)} %bitcast.3, ...), custom_call_target="tpu_custom_call" | custom-call | tf_op jit(solution)/shard_map/macaron/pallas_call | solution.py:450
  60.1 1.7 %copy.12 = bf16[128,1024]{1,0:T(8,128)(2,1)} copy(bf16[128,1024]{1,0:T(8,128)(2,1)} %macaron.1) | data formatting | bytes 524288
